TPU v7x, 32 devices: a whole 2x2x4 slice. The times are simulated.
32 devices in a mesh: grp: 2 (over y), tp: 4 (over z), dp: 4 (over x, core).
Axes of the slice: x: 2, y: 2, z: 4, core: 2. Of those that a mesh axis runs over, the one named last changes fastest.
Arguments:
- tokens: bfloat16 [128, 8, 2048], P('grp', None, 'dp'), parts along dimension 0, may hold values from -64 to 64
- live_counts: int32 [128], P(('grp', 'dp')), parts along dimension 0, may hold values from 1 to 8, 256 in all
- norm_gain: float32 [2, 2048], P(None, 'dp'), may hold values from 0.1 to 1.9
- w_branch: bfloat16 [2, 2048, 4096], P(None, 'dp', 'tp'), may hold values from -0.125 to 0.125
- w_silu_gate: bfloat16 [2, 2048, 4096], P(None, 'dp', 'tp'), may hold values from -0.125 to 0.125
- conv_weight: float32 [2, 4, 4096], P(None, None, 'tp'), may hold values from -3 to 3
- w_query: bfloat16 [2, 16, 256, 256], P(None, 'tp'), may hold values from -0.375 to 0.375
- w_key: bfloat16 [2, 16, 256, 256], P(None, 'tp'), may hold values from -0.375 to 0.375
- w_value: bfloat16 [2, 16, 256, 256], P(None, 'tp'), may hold values from -0.375 to 0.375
- w_input_gate: bfloat16 [2, 16, 768], P(None, 'tp'), may hold values from -0.21875 to 0.21875
- w_forget_gate: bfloat16 [2, 16, 768], P(None, 'tp'), may hold values from -0.21875 to 0.21875
- bias_input: float32 [2, 16], P(None, 'tp'), may hold values from -2 to 2
- bias_forget: float32 [2, 16], P(None, 'tp'), may hold values from -1 to 5
- out_gain: float32 [2, 16, 256], P(None, 'tp'), may hold values from 0.25 to 4
- skip_gain: float32 [2, 4096], P(None, 'tp'), may hold values from 0.25 to 4
- w_out: bfloat16 [2, 4096, 2048], P(None, 'tp', 'dp'), may hold values from -0.09375 to 0.09375
- conv_state: bfloat16 [2, 128, 3, 4096], P(None, ('grp', 'dp'), None, 'tp'), parts along dimension 1, may hold values from -6 to 6
- memory: float32 [2, 128, 16, 256, 256], P(None, ('grp', 'dp'), 'tp'), parts along dimension 1, may hold values from -0.375 to 0.375
- max_state: float32 [2, 128, 16], P(None, ('grp', 'dp'), 'tp'), parts along dimension 1, may hold values from -4 to 4
Outputs:
- out_tokens: bfloat16 [128, 8, 2048], P('grp', None, 'dp'), parts along dimension 0
- new_conv_state: bfloat16 [2, 128, 3, 4096], P(None, ('grp', 'dp'), None, 'tp'), parts along dimension 1
- new_memory: float32 [2, 128, 16, 256, 256], P(None, ('grp', 'dp'), 'tp'), parts along dimension 1
- new_max: float32 [2, 128, 16], P(None, ('grp', 'dp'), 'tp'), parts along dimension 1
There are 2 independent parts, one for each index of `grp`. A program takes and returns all parts, laid end to end along the dimension named above; an argument that names none is the same for every part. Nothing has to cross between parts.
Inputs may be any that keep to these rules, and one draw needn't show every extreme that they name: `live_counts`: each sequence has at least one live slot; within each part (each independent copy of the problem) the 64 counts sum to 256, so the whole array sums to that times the number of parts; in each part some sequence uses all 8 slots.
All inputs are finite; a program needn't handle non-finite values. No bound on the sum of `live_counts` on one device may be relied on, other than what follows from the above.
Results may differ from a plain program's by a relative error of at most 0.035.
Values may be sent and summed in bfloat16 or wider, within the bound.
A program may use at most 192 MiB of HBM per device.

v0:
```python
import jax
import jax.numpy as jnp
from jax import lax
from jax.sharding import PartitionSpec as P

D = 2048
HEAD_DIM = 256
CONV = 4
LAYERS = 2
epsilon = 1e-06
very_negative = -1e30


def recurrent_cell(
    branch,
    silu_gate,
    live_counts,
    conv_weight,
    w_query,
    w_key,
    w_value,
    w_input_gate,
    w_forget_gate,
    bias_input,
    bias_forget,
    out_gain,
    skip_gain,
    conv_state,
    memory,
    max_state,
):
    local_batch = branch.shape[0]
    steps = branch.shape[1]
    local_width = branch.shape[2]
    local_heads = w_query.shape[0]
    padded = jnp.concatenate([conv_state, branch], axis=1)
    conv_sum = jnp.zeros((local_batch, steps, local_width), jnp.float32)
    for offset in range(CONV):
        conv_sum = (
            conv_sum + padded[:, offset : offset + steps].astype(jnp.float32) * conv_weight[offset]
        )
    convolved = jax.nn.silu(conv_sum).astype(jnp.bfloat16)
    picks = live_counts[:, None] + jnp.arange(CONV - 1, dtype=jnp.int32)[None, :]
    new_conv = jnp.take_along_axis(padded, picks[:, :, None], axis=1)
    conv_heads = convolved.reshape(local_batch, steps, local_heads, HEAD_DIM)
    branch_heads = branch.reshape(local_batch, steps, local_heads, HEAD_DIM)
    queries = jnp.einsum(
        "blhd,hde->blhe", conv_heads, w_query, preferred_element_type=jnp.float32
    ).astype(jnp.bfloat16)
    key_rows = jnp.einsum(
        "blhd,hde->blhe", conv_heads, w_key, preferred_element_type=jnp.float32
    ).astype(jnp.bfloat16)
    value_rows = jnp.einsum(
        "blhd,hde->blhe", branch_heads, w_value, preferred_element_type=jnp.float32
    ).astype(jnp.bfloat16)
    joined = jnp.concatenate([queries, key_rows, value_rows], axis=-1)
    input_log = (
        jnp.einsum("blhc,hc->blh", joined, w_input_gate, preferred_element_type=jnp.float32)
        + bias_input
    )
    forget_pre = (
        jnp.einsum("blhc,hc->blh", joined, w_forget_gate, preferred_element_type=jnp.float32)
        + bias_forget
    )
    forget_log = jax.nn.log_sigmoid(forget_pre)
    positions = jnp.arange(steps, dtype=jnp.int32)
    live = positions[None, :] < live_counts[:, None]
    input_log = jnp.transpose(jnp.where(live[:, :, None], input_log, very_negative), (0, 2, 1))
    forget_log = jnp.transpose(jnp.where(live[:, :, None], forget_log, 0.0), (0, 2, 1))
    query_heads = jnp.transpose(queries.astype(jnp.float32), (0, 2, 1, 3))
    key_heads = jnp.transpose(key_rows.astype(jnp.float32), (0, 2, 1, 3)) * HEAD_DIM ** (-0.5)
    value_heads = jnp.transpose(value_rows.astype(jnp.float32), (0, 2, 1, 3))
    cumulative = jnp.cumsum(forget_log, axis=-1)
    log_weights = cumulative[..., :, None] - cumulative[..., None, :] + input_log[..., None, :]
    causal = positions[:, None] >= positions[None, :]
    log_weights = jnp.where(causal, log_weights, very_negative)
    carried = cumulative + max_state[..., None]
    stabilizer = jnp.maximum(jnp.max(log_weights, axis=-1), carried)
    weights = jnp.exp(log_weights - stabilizer[..., None])
    carried_scale = jnp.exp(carried - stabilizer)
    scores = jnp.einsum("bhtd,bhsd->bhts", query_heads, key_heads) * weights
    numerator = jnp.einsum("bhts,bhse->bhte", scores, value_heads)
    numerator = numerator + carried_scale[..., None] * jnp.einsum(
        "bhtd,bhde->bhte", query_heads, memory
    )
    centered = numerator - jnp.mean(numerator, axis=-1, keepdims=True)
    normalized = centered * lax.rsqrt(
        jnp.mean(centered * centered, axis=-1, keepdims=True) + epsilon
    )
    normalized = normalized * out_gain[None, :, None, :]
    readout = jnp.transpose(normalized, (0, 2, 1, 3)).reshape(local_batch, steps, local_width)
    new_max = stabilizer[..., -1]
    decay = jnp.exp(cumulative[..., -1] + max_state - new_max)
    update_weight = jnp.exp(cumulative[..., -1:] - cumulative + input_log - new_max[..., None])
    new_memory = decay[..., None, None] * memory + jnp.einsum(
        "bhs,bhsd,bhse->bhde", update_weight, key_heads, value_heads
    )
    mixed = (readout + skip_gain * convolved.astype(jnp.float32)) * jax.nn.silu(
        silu_gate.astype(jnp.float32)
    )
    mixed = jnp.where(live[:, :, None], mixed, 0.0).astype(jnp.bfloat16)
    return (mixed, new_conv, new_memory, new_max)


def layer_step(
    tokens,
    live_counts,
    gain,
    w_branch,
    w_silu_gate,
    conv_weight,
    w_query,
    w_key,
    w_value,
    w_input_gate,
    w_forget_gate,
    bias_input,
    bias_forget,
    out_gain,
    skip_gain,
    w_out,
    conv_state,
    memory,
    max_state,
):
    all_batch = tokens.shape[0]
    steps = tokens.shape[1]
    local_features = tokens.shape[2]
    local_width = w_branch.shape[1]
    local_batch = live_counts.shape[0]
    floats = tokens.astype(jnp.float32)
    partial_squares = jnp.sum(floats * floats, axis=-1)
    total_squares = lax.psum(partial_squares, "dp")
    normed = (floats * lax.rsqrt(total_squares / D + epsilon)[..., None] * gain).astype(
        jnp.bfloat16
    )
    rows = normed.reshape(local_batch * lax.axis_size("dp") * steps, local_features)
    first = jnp.dot(rows, w_branch, preferred_element_type=jnp.float32)
    second = jnp.dot(rows, w_silu_gate, preferred_element_type=jnp.float32)
    summed = lax.psum_scatter(
        jnp.stack([first, second], axis=1)
        .reshape(local_batch * lax.axis_size("dp"), steps, 2, local_width)
        .astype(jnp.bfloat16),
        "dp",
        scatter_dimension=0,
        tiled=True,
    ).astype(jnp.float32)
    branch = summed[:, :, 0].astype(jnp.bfloat16)
    silu_gate = summed[:, :, 1].astype(jnp.bfloat16)
    mixed, new_conv, new_memory, new_max = recurrent_cell(
        branch,
        silu_gate,
        live_counts,
        conv_weight,
        w_query,
        w_key,
        w_value,
        w_input_gate,
        w_forget_gate,
        bias_input,
        bias_forget,
        out_gain,
        skip_gain,
        conv_state,
        memory,
        max_state,
    )
    piece = lax.all_gather(mixed, "dp", axis=0, tiled=True)
    flat = piece.reshape(piece.shape[0] * steps, local_width)
    product = jnp.dot(flat, w_out, preferred_element_type=jnp.float32)
    terms = product.reshape(piece.shape[0], steps, local_features)
    flat_terms = terms.reshape(all_batch * steps, local_features)
    share = lax.psum_scatter(
        flat_terms.astype(jnp.bfloat16), "tp", scatter_dimension=0, tiled=True
    ).astype(jnp.float32)
    share_rows = share.shape[0]
    residual_rows = lax.dynamic_slice_in_dim(
        floats.reshape(all_batch * steps, local_features),
        lax.axis_index("tp") * share_rows,
        share_rows,
        0,
    )
    new_share = (residual_rows + share.astype(jnp.bfloat16).astype(jnp.float32)).astype(
        jnp.bfloat16
    )
    result = lax.all_gather(new_share, "tp", axis=0, tiled=True).reshape(
        all_batch, steps, local_features
    )
    return (result, new_conv, new_memory, new_max)


def per_device(
    tokens,
    live_counts,
    norm_gain,
    w_branch,
    w_silu_gate,
    conv_weight,
    w_query,
    w_key,
    w_value,
    w_input_gate,
    w_forget_gate,
    bias_input,
    bias_forget,
    out_gain,
    skip_gain,
    w_out,
    conv_state,
    memory,
    max_state,
):
    stream = tokens
    conv_list = []
    memory_list = []
    max_list = []
    for which_layer in range(LAYERS):
        stream, new_conv, new_memory, new_max = layer_step(
            stream,
            live_counts,
            norm_gain[which_layer],
            w_branch[which_layer],
            w_silu_gate[which_layer],
            conv_weight[which_layer],
            w_query[which_layer],
            w_key[which_layer],
            w_value[which_layer],
            w_input_gate[which_layer],
            w_forget_gate[which_layer],
            bias_input[which_layer],
            bias_forget[which_layer],
            out_gain[which_layer],
            skip_gain[which_layer],
            w_out[which_layer],
            conv_state[which_layer],
            memory[which_layer],
            max_state[which_layer],
        )
        conv_list.append(new_conv)
        memory_list.append(new_memory)
        max_list.append(new_max)
    return (stream, jnp.stack(conv_list), jnp.stack(memory_list), jnp.stack(max_list))


def solution(mesh):
    in_specs = (
        P("grp", None, "dp"),
        P(("grp", "dp")),
        P(None, "dp"),
        P(None, "dp", "tp"),
        P(None, "dp", "tp"),
        P(None, None, "tp"),
        P(None, "tp", None, None),
        P(None, "tp", None, None),
        P(None, "tp", None, None),
        P(None, "tp", None),
        P(None, "tp", None),
        P(None, "tp"),
        P(None, "tp"),
        P(None, "tp", None),
        P(None, "tp"),
        P(None, "tp", "dp"),
        P(None, ("grp", "dp"), None, "tp"),
        P(None, ("grp", "dp"), "tp", None, None),
        P(None, ("grp", "dp"), "tp"),
    )
    out_specs = (
        P("grp", None, "dp"),
        P(None, ("grp", "dp"), None, "tp"),
        P(None, ("grp", "dp"), "tp", None, None),
        P(None, ("grp", "dp"), "tp"),
    )
    return jax.shard_map(
        per_device, mesh=mesh, in_specs=in_specs, out_specs=out_specs, check_vma=False
    )
```

profile of v0, /device:TPU:0, one launch (start us, length us, event | category | flops | bytes accessed | tf_op | source)
XLA Modules:
  0.0 297.1 jit_solution(8914190688373300822)
XLA Ops:
  7.2 1.4 fusion.162
  8.7 1.2 fusion.16
  9.9 12.9 %psum.14 = f32[64,8]{1,0:T(8,128)S(1)} all-reduce(f32[64,8]{1,0:T(8,128)S(1)} %fusion.16), channel_id=1, replica_groups=mesh['grp'=2,'tp'=4,'dp'=4] {'dp'}, use_global_device_ids=true, to_apply=%region_1.0 | all-reduce | flops 512 | bytes 4096 | tf_op jit(solution)/shard_map/psum | solution.py:133
  22.8 2.1 fusion.11
  25.0 0.8 fusion.10
  26.2 2.5 copy.279
  29.5 0.6 slice_bitcast_fusion.8
  30.1 0.5 slice_bitcast_fusion.10
  30.7 0.6 slice_bitcast_fusion.11
  31.3 0.6 slice_bitcast_fusion.6
  31.9 0.6 fusion.161
  32.5 0.6 slice_bitcast_fusion.2
  33.1 0.6 slice_bitcast_fusion.3
  33.7 0.6 fusion.160
  34.3 26.1 %reduce-scatter.15.cloned.1.call-done = bf16[16,16384]{1,0:T(8,128)(2,1)} async-done(((bf16[64,16384]{1,0:T(8,128)(2,1)}), bf16[16,16384]{1,0:T(8,128)(2,1)}) %reduce-scatter.15.cloned.1.call-update) | async-done | bytes 524304
  60.5 1.4 copy.280
  62.1 0.9 reshape.308
  63.7 1.4 convolution_convert_fusion.10
  65.6 1.8 fusion.76
  67.4 1.8 fusion.77
  69.4 2.8 reduce_window_sum.17
  73.6 0.8 exponential_multiply_fusion.1
  74.4 0.8 bitcast_multiply_fusion.6
  75.2 7.0 %fusion.4 = f32[16,4,8,256]{3,2,1,0:T(8,128)S(1)} fusion(f32[2,16,4,256,256]{4,3,2,1,0:T(8,128)} %param.38, bf16[4,16,8,256]{3,2,1,0:T(8,128)(2,1)S(1)} %convolution_convert_fusion.11), kind=kOutput, calls=%fused_computation.9 | convolution fusion | flops 67108864 | bytes 9175040 | tf_op jit(solution)/shard_map/bhtd,bhde->bhte/dot_general | solution.py:83
  82.2 1.4 fusion.108
  84.3 0.5 fusion.71
  84.8 0.9 copy.214
  85.8 16.8 %all-gather.3.cloned.1.call-done = bf16[64,8,1024]{2,1,0:T(8,128)(2,1)} async-done(((bf16[16,8,1024]{2,1,0:T(8,128)(2,1)}), bf16[64,8,1024]{2,1,0:T(8,128)(2,1)}) %all-gather.3.cloned.1.call-update) | async-done | bytes 1048592 | tf_op jit(solution)/shard_map/all_gather | solution.py:168
  102.6 3.0 %convolution_convert_fusion.5 = bf16[512,512]{1,0:T(8,128)(2,1)} fusion(bf16[64,8,1024]{2,1,0:T(8,128)(2,1)} %all-gather.3.cloned.1.call-done, bf16[2,1024,512]{2,1,0:T(8,128)(2,1)} %param.36), kind=kOutput, calls=%fused_computation.29 | convolution fusion | flops 537133056 | bytes 2621440 | tf_op jit(solution)/shard_map/dot_general | solution.py:170
  105.8 21.8 %reduce-scatter.11.cloned.1.call-done = bf16[128,512]{1,0:T(8,128)(2,1)} async-done(((bf16[512,512]{1,0:T(8,128)(2,1)}), bf16[128,512]{1,0:T(8,128)(2,1)}) %reduce-scatter.11.cloned.1.call-update) | async-done | bytes 131088 | tf_op jit(solution)/shard_map/reduce_scatter | solution.py:173
  127.6 0.9 add_convert_fusion.1
  128.6 15.6 %all_gather.13 = bf16[512,512]{1,0:T(8,128)(2,1)S(1)} all-gather(bf16[128,512]{1,0:T(8,128)(2,1)S(1)} %add_convert_fusion.1), channel_id=1, replica_groups=mesh['grp'=2,'tp'=4,'dp'=4] {'tp'}, dimensions={0}, use_global_device_ids=true | all-gather | bytes 655360 | tf_op jit(solution)/shard_map/all_gather | solution.py:186
  144.4 10.3 %psum.15 = f32[64,8]{1,0:T(8,128)S(1)} all-reduce(f32[64,8]{1,0:T(8,128)S(1)} %reduce_sum.60), channel_id=1, replica_groups=mesh['grp'=2,'tp'=4,'dp'=4] {'dp'}, use_global_device_ids=true, to_apply=%region_9.10 | all-reduce | flops 512 | bytes 4096 | tf_op jit(solution)/shard_map/psum | solution.py:133
  154.8 2.0 fusion.13
  156.8 2.0 fusion.12
  159.2 2.5 copy.281
  161.8 0.6 copy-done.46
  162.4 0.7 copy.228
  163.5 28.2 %reduce-scatter.17.cloned.1.call-done = bf16[16,16384]{1,0:T(8,128)(2,1)} async-done(((bf16[64,16384]{1,0:T(8,128)(2,1)}), bf16[16,16384]{1,0:T(8,128)(2,1)}) %reduce-scatter.17.cloned.1.call-update) | async-done | bytes 524304
  191.6 1.4 copy.282
  193.0 0.7 fusion.158
  193.9 0.9 reshape.309
  195.3 1.4 convolution_convert_fusion.8
  196.8 1.4 convolution_convert_fusion.7
  198.2 1.5 convolution_convert_fusion.6
  199.8 1.8 fusion.74
  201.6 1.8 fusion.75
  203.6 2.8 reduce_window_sum.18
  207.1 7.1 %fusion = f32[16,4,8,256]{3,2,1,0:T(8,128)S(1)} fusion(f32[2,16,4,256,256]{4,3,2,1,0:T(8,128)} %param.38, bf16[4,16,8,256]{3,2,1,0:T(8,128)(2,1)} %copy-done.1), kind=kOutput, calls=%fused_computation.4 | convolution fusion | flops 67108864 | bytes 9175040 | tf_op jit(solution)/shard_map/bhtd,bhde->bhte/dot_general | solution.py:83
  214.2 1.2 gather_fusion
  215.4 1.2 gather_fusion.1
  217.1 0.8 copy.250
  218.7 1.7 bitcast_multiply_fusion.3
  220.4 1.5 fusion.109
  222.9 0.5 fusion.70
  223.4 0.9 copy.227
  224.5 0.6 pad_maximum_fusion.12
  225.1 10.8 %fusion.3 = f32[1,16,4,256,256]{4,3,2,1,0:T(8,128)} fusion(f32[2,16,4,256,256]{4,3,2,1,0:T(8,128)} %param.38, f32[16,4]{1,0:T(8,128)S(1)} %copy.242, bf16[16,4,8,256]{3,2,0,1:T(8,128)(2,1)S(1)} %get-tuple-element.27, bf16[4,16,8,256]{3,2,1,0:T(8,128)(2,1)S(1)} %copy-done.9), kind=kOutput, calls=%fused_computation.7 | convolution fusion | flops 75497472 | bytes 34078976 | tf_op jit(solution)/shard_map/bhs,bhsd,bhse->bhde/dot_general | solution.py:95
  236.0 10.8 %fusion.7 = f32[1,16,4,256,256]{4,3,2,1,0:T(8,128)} fusion(f32[2,16,4,256,256]{4,3,2,1,0:T(8,128)} %param.38, f32[16,4]{1,0:T(8,128)S(1)} %copy.234, bf16[16,4,8,256]{3,2,0,1:T(8,128)(2,1)S(1)} %get-tuple-element.25, bf16[4,16,8,256]{3,2,1,0:T(8,128)(2,1)S(1)} %copy-done.7), kind=kOutput, calls=%fused_computation.12 | convolution fusion | flops 75497472 | bytes 34078976 | tf_op jit(solution)/shard_map/bhs,bhsd,bhse->bhde/dot_general | solution.py:95
  246.8 3.0 %convolution_convert_fusion.4 = bf16[512,512]{1,0:T(8,128)(2,1)} fusion(bf16[64,8,1024]{2,1,0:T(8,128)(2,1)} %all-gather.5.cloned.1.call-done, bf16[2,1024,512]{2,1,0:T(8,128)(2,1)} %param.36), kind=kOutput, calls=%fused_computation.28 | convolution fusion | flops 537133056 | bytes 2621440 | tf_op jit(solution)/shard_map/dot_general | solution.py:170
  249.9 23.1 %pad_maximum_fusion = f32[2,16,4,256,256]{4,3,2,1,0:T(8,128)} fusion(f32[1,16,4,256,256]{4,3,2,1,0:T(8,128)} %fusion.3, f32[1,16,4,256,256]{4,3,2,1,0:T(8,128)} %fusion.7), kind=kLoop, calls=%fused_computation.2 | loop fusion | flops 8388608 | bytes 67108864 | tf_op jit(solution)/shard_map/stack | solution.py:242
  273.0 0.9 add_convert_fusion
  273.9 15.6 %all_gather.15 = bf16[512,512]{1,0:T(8,128)(2,1)S(1)} all-gather(bf16[128,512]{1,0:T(8,128)(2,1)S(1)} %add_convert_fusion), channel_id=1, replica_groups=mesh['grp'=2,'tp'=4,'dp'=4] {'tp'}, dimensions={0}, use_global_device_ids=true | all-gather | bytes 655360 | tf_op jit(solution)/shard_map/all_gather | solution.py:186
  289.5 0.8 copy.380
  (184 shorter events, 10.2 us)
Async XLA Ops:
  7.2 17.8 %copy-start = (bf16[64,8,512]{2,1,0:T(8,128)(2,1)S(1)}, bf16[64,8,512]{2,1,0:T(8,128)(2,1)}, u32[]{:S(2)}) copy-start(bf16[64,8,512]{2,1,0:T(8,128)(2,1)} %param.21) | copy-start | bytes 1572868
  7.2 17.8 %copy-start.47 = (bf16[2,512,1024]{2,1,0:T(8,128)(2,1)S(1)}, bf16[2,512,1024]{2,1,0:T(8,128)(2,1)}, u32[]{:S(2)}) copy-start(bf16[2,512,1024]{2,1,0:T(8,128)(2,1)} %param.24) | copy-start | bytes 6291460
  7.2 53.3 %reduce-scatter.15.cloned.1.call-start = ((), (), s32[]{:S(2)}) async-start(), calls=%async_computation.8 | async-start | bytes 2621440
  28.7 0.7 copy-start.45
  28.7 0.8 copy-start.24
  28.7 1.4 copy-start.43
  28.7 2.0 copy-start.44
  28.7 2.6 copy-start.32
  28.7 3.2 %copy-start.33 = (f32[2,1024]{1,0:T(2,128)S(1)}, f32[2,1024]{1,0:T(2,128)}, u32[]{:S(2)}) copy-start(f32[2,1024]{1,0:T(2,128)} %param.35) | copy-start | bytes 24580
  28.7 3.7 %copy-start.26 = (bf16[2,4,768]{2,1,0:T(4,128)(2,1)S(1)}, bf16[2,4,768]{2,1,0:T(4,128)(2,1)}, u32[]{:S(2)}) copy-start(bf16[2,4,768]{2,1,0:T(4,128)(2,1)} %param.30) | copy-start | bytes 36868
  28.7 4.3 %copy-start.27 = (bf16[2,4,768]{2,1,0:T(4,128)(2,1)S(1)}, bf16[2,4,768]{2,1,0:T(4,128)(2,1)}, u32[]{:S(2)}) copy-start(bf16[2,4,768]{2,1,0:T(4,128)(2,1)} %param.31) | copy-start | bytes 36868
  28.8 4.9 %copy-start.14 = (f32[2,4,1024]{2,1,0:T(4,128)S(1)}, f32[2,4,1024]{2,1,0:T(4,128)}, u32[]{:S(2)}) copy-start(f32[2,4,1024]{2,1,0:T(4,128)} %param.26) | copy-start | bytes 98308
  28.8 5.5 %copy-start.11 = (bf16[2,16,3,1024]{3,1,2,0:T(8,128)(2,1)S(1)}, bf16[2,16,3,1024]{3,1,2,0:T(8,128)(2,1)}, u32[]{:S(2)}) copy-start(bf16[2,16,3,1024]{3,1,2,0:T(8,128)(2,1)} %param.37) | copy-start | bytes 589828
  28.8 73.8 %all-gather.3.cloned.1.call-start = ((), (), s32[]{:S(2)}) async-start(), calls=%async_computation.4 | async-start | bytes 1310720 | tf_op jit(solution)/shard_map/all_gather | solution.py:168
  29.4 32.5 %copy-start.28 = (pred[16,8]{0,1:T(8,128)(4,1)}, pred[16,8]{0,1:T(8,128)(4,1)S(1)}, u32[]{:S(2)}) copy-start(pred[16,8]{0,1:T(8,128)(4,1)S(1)} %iota_compare_fusion.1) | copy-start | bytes 388
  30.1 42.2 %copy-start.39 = (pred[8,8]{1,0:T(8,128)(4,1)}, pred[8,8]{1,0:T(8,128)(4,1)S(1)}, u32[]{:S(2)}) copy-start(pred[8,8]{1,0:T(8,128)(4,1)S(1)} %iota_compare_fusion) | copy-start | bytes 196
  30.7 41.6 %copy-start.38 = (f32[4]{0:T(128)}, f32[4]{0:T(128)S(1)}, u32[]{:S(2)}) copy-start(f32[4]{0:T(128)S(1)} %get-tuple-element.66) | copy-start | bytes 52
  60.5 3.0 copy-start.3
  63.4 1.7 copy-start.10
  63.4 1.7 copy-start.48
  65.6 16.6 %copy-start.6 = (bf16[4,16,8,256]{3,2,1,0:T(8,128)(2,1)}, bf16[4,16,8,256]{3,2,1,0:T(8,128)(2,1)S(1)}, u32[]{:S(2)}) copy-start(bf16[4,16,8,256]{3,2,1,0:T(8,128)(2,1)S(1)} %convolution_convert_fusion.9) | copy-start | bytes 786436
  72.3 0.6 copy-start.12
  73.5 8.7 %copy-start.15 = (f32[16,4,1]{0,1,2:T(4,128)}, f32[16,4,1]{0,1,2:T(4,128)S(1)}, u32[]{:S(2)}) copy-start(f32[16,4,1]{0,1,2:T(4,128)S(1)} %copy.232) | copy-start | bytes 772
  75.2 7.0 %copy-start.13 = (f32[16,4,8]{2,1,0:T(4,128)S(1)}, f32[16,4,8]{2,1,0:T(4,128)}, u32[]{:S(2)}) copy-start(f32[16,4,8]{2,1,0:T(4,128)} %copy-done.12) | copy-start | bytes 6148
  82.2 1.8 copy-start.23
  83.6 0.7 copy-start.29
  85.7 41.9 %reduce-scatter.11.cloned.1.call-start = ((), (), s32[]{:S(2)}) async-start(), calls=%async_computation.5 | async-start | bytes 655360 | tf_op jit(solution)/shard_map/reduce_scatter | solution.py:173
  105.6 49.1 %copy-start.42 = (f32[1,512]{1,0:T(1,128)S(1)}, f32[1,512]{1,0:T(1,128)}, u32[]{:S(2)}) copy-start(f32[1,512]{1,0:T(1,128)} %get-tuple-element.60) | copy-start | bytes 6148
  105.6 86.0 %reduce-scatter.17.cloned.1.call-start = ((), (), s32[]{:S(2)}) async-start(), calls=%async_computation.9 | async-start | bytes 2621440
  161.7 0.7 copy-start.46
  161.7 1.3 copy-start.34
  161.7 85.1 %all-gather.5.cloned.1.call-start = ((), (), s32[]{:S(2)}) async-start(), calls=%async_computation.6 | async-start | bytes 1310720 | tf_op jit(solution)/shard_map/all_gather | solution.py:168
  191.6 3.2 %copy-start.17 = (f32[1,1,1024]{2,1,0:T(1,128)S(1)}, f32[1,1,1024]{2,1,0:T(1,128)}, u32[]{:S(2)}) copy-start(f32[1,1,1024]{2,1,0:T(1,128)} %get-tuple-element.37) | copy-start | bytes 12292
  191.6 3.2 %copy-start.18 = (f32[1,1,1024]{2,1,0:T(1,128)S(1)}, f32[1,1,1024]{2,1,0:T(1,128)}, u32[]{:S(2)}) copy-start(f32[1,1,1024]{2,1,0:T(1,128)} %get-tuple-element.38) | copy-start | bytes 12292
  191.6 3.2 %copy-start.19 = (f32[1,1,1024]{2,1,0:T(1,128)S(1)}, f32[1,1,1024]{2,1,0:T(1,128)}, u32[]{:S(2)}) copy-start(f32[1,1,1024]{2,1,0:T(1,128)} %get-tuple-element.43) | copy-start | bytes 12292
  191.6 3.2 %copy-start.20 = (f32[1,1,1024]{2,1,0:T(1,128)S(1)}, f32[1,1,1024]{2,1,0:T(1,128)}, u32[]{:S(2)}) copy-start(f32[1,1,1024]{2,1,0:T(1,128)} %get-tuple-element.44) | copy-start | bytes 12292
  195.1 4.6 %copy-start.35 = (bf16[4,768,1,1]{1,0,2,3:T(4,128)(2,1)S(1)}, bf16[4,768,1,1]{1,0,2,3:T(4,128)(2,1)}, u32[]{:S(2)}) copy-start(bf16[4,768,1,1]{1,0,2,3:T(4,128)(2,1)} %get-tuple-element.49) | copy-start | bytes 18436
  195.3 2.9 copy-start.49
  196.7 4.8 %copy-start.1 = (bf16[4,16,8,256]{3,2,1,0:T(8,128)(2,1)}, bf16[4,16,8,256]{3,2,1,0:T(8,128)(2,1)S(1)}, u32[]{:S(2)}) copy-start(bf16[4,16,8,256]{3,2,1,0:T(8,128)(2,1)S(1)} %convolution_convert_fusion.8) | copy-start | bytes 786436
  198.2 5.2 %copy-start.4 = (bf16[4,16,8,256]{3,2,1,0:T(8,128)(2,1)}, bf16[4,16,8,256]{3,2,1,0:T(8,128)(2,1)S(1)}, u32[]{:S(2)}) copy-start(bf16[4,16,8,256]{3,2,1,0:T(8,128)(2,1)S(1)} %convolution_convert_fusion.7) | copy-start | bytes 786436
  198.2 3.4 %copy-start.36 = (bf16[4,768,1,1]{1,0,2,3:T(4,128)(2,1)S(1)}, bf16[4,768,1,1]{1,0,2,3:T(4,128)(2,1)}, u32[]{:S(2)}) copy-start(bf16[4,768,1,1]{1,0,2,3:T(4,128)(2,1)} %get-tuple-element.47) | copy-start | bytes 18436
  199.7 3.7 %copy-start.8 = (bf16[4,16,8,256]{3,2,1,0:T(8,128)(2,1)}, bf16[4,16,8,256]{3,2,1,0:T(8,128)(2,1)S(1)}, u32[]{:S(2)}) copy-start(bf16[4,16,8,256]{3,2,1,0:T(8,128)(2,1)S(1)} %convolution_convert_fusion.6) | copy-start | bytes 786436
  199.7 3.7 %copy-start.41 = (f32[4]{0:T(128)S(1)}, f32[4]{0:T(128)}, u32[]{:S(2)}) copy-start(f32[4]{0:T(128)} %get-tuple-element.63) | copy-start | bytes 52
  199.7 6.7 %copy-start.37 = (f32[4]{0:T(128)S(1)}, f32[4]{0:T(128)}, u32[]{:S(2)}) copy-start(f32[4]{0:T(128)} %get-tuple-element.65) | copy-start | bytes 52
  199.8 6.7 %copy-start.40 = (pred[8,8]{1,0:T(8,128)(4,1)S(1)}, pred[8,8]{1,0:T(8,128)(4,1)}, u32[]{:S(2)}) copy-start(pred[8,8]{1,0:T(8,128)(4,1)} %copy-done.39) | copy-start | bytes 196
  214.1 2.6 copy-start.31
  214.1 4.1 %copy-start.16 = (f32[16,4,1]{0,1,2:T(4,128)S(1)}, f32[16,4,1]{0,1,2:T(4,128)}, u32[]{:S(2)}) copy-start(f32[16,4,1]{0,1,2:T(4,128)} %copy-done.15) | copy-start | bytes 772
  214.2 4.1 %copy-start.25 = (f32[2,16,4]{1,2,0:T(4,128)S(1)}, f32[2,16,4]{1,2,0:T(4,128)}, u32[]{:S(2)}) copy-start(f32[2,16,4]{1,2,0:T(4,128)} %param.39) | copy-start | bytes 1540
  215.4 5.0 %copy-start.2 = (bf16[4,16,8,256]{3,2,1,0:T(8,128)(2,1)S(1)}, bf16[4,16,8,256]{3,2,1,0:T(8,128)(2,1)}, u32[]{:S(2)}) copy-start(bf16[4,16,8,256]{3,2,1,0:T(8,128)(2,1)} %copy-done.1) | copy-start | bytes 786436
  220.4 1.9 copy-start.22
  221.9 1.0 copy-start.5
  221.9 0.9 copy-start.21
  221.9 0.9 copy-start.30
  222.3 2.8 copy-start.9
  224.3 48.7 %reduce-scatter.13.cloned.1.call-start = ((), (), s32[]{:S(2)}) async-start(), calls=%async_computation.7 | async-start | bytes 655360 | tf_op jit(solution)/shard_map/reduce_scatter | solution.py:173
  225.1 10.9 %copy-start.7 = (bf16[4,16,8,256]{3,2,1,0:T(8,128)(2,1)S(1)}, bf16[4,16,8,256]{3,2,1,0:T(8,128)(2,1)}, u32[]{:S(2)}) copy-start(bf16[4,16,8,256]{3,2,1,0:T(8,128)(2,1)} %copy-done.6) | copy-start | bytes 786436
Sparse Core Ops, SparseCore 0:
  28.9 31.4 reduce-scatter.14
  85.8 16.6 all-gather.2
  105.8 21.8 reduce-scatter.10
  161.9 29.7 reduce-scatter.16
  224.4 16.7 all-gather.4
  250.0 21.9 reduce-scatter.12
where the time goes:
time: 298 us; the launch traced here: 297 us
  waiting for transfers between devices  93 us (31%)
  matrix products  65.3 us (22%)
  blocking collectives  54.3 us (18%)
  other arithmetic  41.4 us (14%)
  local copies, waits for them, and re-layouts  27.7 us (9%)
  between operations  15 us (5%)
    unnamed x8, waiting for transfers between devices  54.4 us
    all_gather x2, blocking collectives, layer_step(): lax.all_gather(new_share, 'tp', axis=0, tiled=True)  31.1 us
    psum x2, blocking collectives, layer_step(): total_squares = lax.psum(partial_squares, 'dp')  23.2 us
    another operation x1, other arithmetic, per_device(): jnp.stack(memory_list)  23.1 us
    reduce_scatter x2, waiting for transfers between devices, layer_step(): lax.psum_scatter(flat_terms.astype(jnp.bfloat16), 'tp', scatter_dimension...  21.8 us
    dot_general x2, matrix products, recurrent_cell(): jnp.einsum('bhs,bhsd,bhse->bhde', update_weight, key_heads, value_heads)  21.7 us
    all_gather x2, waiting for transfers between devices, layer_step(): piece = lax.all_gather(mixed, 'dp', axis=0, tiled=True)  16.8 us
    dot_general x2, matrix products, recurrent_cell(): jnp.einsum('bhtd,bhde->bhte', query_heads, memory)  14 us
  transfers between devices with their start and end apart: 6, of which 4 were waited for; matrix products, arithmetic and copies ran while one was open for 17% of the time, Pallas kernels for 0%

commit v1 on v0

--- a/solution.py
+++ b/solution.py
@@ -9,6 +9,15 @@
 LAYERS = 2
 epsilon = 1e-06
 very_negative = -1e30
+
+
+def added_up(x, axis):
+    peers = lax.axis_size(axis)
+    total, hop = (x, 1)
+    while hop < peers:
+        total = total + lax.ppermute(total, axis, [(i, i ^ hop) for i in range(peers)])
+        hop = 2 * hop
+    return total
 
 
 def recurrent_cell(
@@ -130,7 +139,7 @@
     local_batch = live_counts.shape[0]
     floats = tokens.astype(jnp.float32)
     partial_squares = jnp.sum(floats * floats, axis=-1)
-    total_squares = lax.psum(partial_squares, "dp")
+    total_squares = added_up(partial_squares, "dp")
     normed = (floats * lax.rsqrt(total_squares / D + epsilon)[..., None] * gain).astype(
         jnp.bfloat16
     )

time: 298 us -> 286 us (0.960)
  blocking collectives: 54.3 us -> 31.1 us
  waiting for transfers between devices: 93 us -> 99.3 us
  starting transfers between devices: 0.47 us -> 5.51 us
    psum x2 -> x0, blocking collectives: 23.2 us -> none  [layer_step(): total_squares = lax.psum(partial_squares, 'dp')]
    ppermute x0 -> x4, starting transfers between devices: none -> 5.04 us  [added_up(): lax.ppermute(total, axis, [(i, i ^ hop) for i in range(peers)])]
    ppermute x0 -> x4, waiting for transfers between devices: none -> 4.92 us  [added_up(): lax.ppermute(total, axis, [(i, i ^ hop) for i in range(peers)])]
  transfers between devices with their start and end apart: 6 -> 10, of which waited for: 4 -> 8; matrix products, arithmetic and copies ran while one was open for 17% -> 18% of each run, Pallas kernels for 0% -> 0%
where the time goes in v1:
time: 286 us; the launch traced here: 285 us
  waiting for transfers between devices  99.3 us (35%)
  matrix products  65.4 us (23%)
  other arithmetic  41.5 us (15%)
  blocking collectives  31.1 us (11%)
  local copies, waits for them, and re-layouts  27.5 us (10%)
  between operations  15 us (5%)
  starting transfers between devices  5.51 us (2%)
    unnamed x8, waiting for transfers between devices  55.8 us
    all_gather x2, blocking collectives, layer_step(): lax.all_gather(new_share, 'tp', axis=0, tiled=True)  31.1 us
    another operation x1, other arithmetic, per_device(): jnp.stack(memory_list)  23.1 us
    reduce_scatter x2, waiting for transfers between devices, layer_step(): lax.psum_scatter(flat_terms.astype(jnp.bfloat16), 'tp', scatter_dimension...  21.8 us
    dot_general x2, matrix products, recurrent_cell(): jnp.einsum('bhs,bhsd,bhse->bhde', update_weight, key_heads, value_heads)  21.7 us
    all_gather x2, waiting for transfers between devices, layer_step(): piece = lax.all_gather(mixed, 'dp', axis=0, tiled=True)  16.8 us
    dot_general x2, matrix products, recurrent_cell(): jnp.einsum('bhtd,bhde->bhte', query_heads, memory)  14 us
    unnamed x110, local copies, waits for them, and re-layouts  11.9 us
  transfers between devices with their start and end apart: 10, of which 8 were waited for; matrix products, arithmetic and copies ran while one was open for 18% of the time, Pallas kernels for 0%

profile of v1, /device:TPU:0, one launch (start us, length us, event | category | flops | bytes accessed | tf_op | source)
XLA Modules:
  0.0 285.3 jit_solution(6040385288834833798)
XLA Ops:
  7.2 1.4 fusion.16
  8.6 0.6 collective-permute-start
  9.2 0.9 collective-permute-done
  10.0 2.8 collective-permute-start.1
  12.8 1.3 fusion.162
  14.8 2.1 fusion.11
  16.9 0.8 fusion.10
  18.1 2.5 copy.279
  21.4 0.6 slice_bitcast_fusion.8
  23.1 0.6 slice_bitcast_fusion.6
  23.7 0.6 fusion.161
  24.3 0.6 slice_bitcast_fusion.2
  24.9 0.6 slice_bitcast_fusion.3
  25.5 0.6 fusion.160
  26.1 27.7 %reduce-scatter.15.cloned.1.call-done = bf16[16,16384]{1,0:T(8,128)(2,1)} async-done(((bf16[64,16384]{1,0:T(8,128)(2,1)}), bf16[16,16384]{1,0:T(8,128)(2,1)}) %reduce-scatter.15.cloned.1.call-update) | async-done | bytes 524304
  53.9 1.4 copy.280
  55.5 0.9 reshape.308
  57.1 1.4 convolution_convert_fusion.10
  59.0 1.8 fusion.76
  60.9 1.8 fusion.77
  62.8 2.8 reduce_window_sum.17
  67.0 0.8 exponential_multiply_fusion.1
  67.8 0.8 bitcast_multiply_fusion.6
  68.6 7.0 %fusion.4 = f32[16,4,8,256]{3,2,1,0:T(8,128)S(1)} fusion(f32[2,16,4,256,256]{4,3,2,1,0:T(8,128)} %param.38, bf16[4,16,8,256]{3,2,1,0:T(8,128)(2,1)S(1)} %convolution_convert_fusion.11), kind=kOutput, calls=%fused_computation.9 | convolution fusion | flops 67108864 | bytes 9175040 | tf_op jit(solution)/shard_map/bhtd,bhde->bhte/dot_general | solution.py:92
  75.6 1.4 fusion.108
  78.2 0.9 copy.214
  79.2 16.8 %all-gather.3.cloned.1.call-done = bf16[64,8,1024]{2,1,0:T(8,128)(2,1)} async-done(((bf16[16,8,1024]{2,1,0:T(8,128)(2,1)}), bf16[64,8,1024]{2,1,0:T(8,128)(2,1)}) %all-gather.3.cloned.1.call-update) | async-done | bytes 1048592 | tf_op jit(solution)/shard_map/all_gather | solution.py:177
  96.0 3.0 %convolution_convert_fusion.5 = bf16[512,512]{1,0:T(8,128)(2,1)} fusion(bf16[64,8,1024]{2,1,0:T(8,128)(2,1)} %all-gather.3.cloned.1.call-done, bf16[2,1024,512]{2,1,0:T(8,128)(2,1)} %param.36), kind=kOutput, calls=%fused_computation.29 | convolution fusion | flops 537133056 | bytes 2621440 | tf_op jit(solution)/shard_map/dot_general | solution.py:179
  99.2 21.8 %reduce-scatter.11.cloned.1.call-done = bf16[128,512]{1,0:T(8,128)(2,1)} async-done(((bf16[512,512]{1,0:T(8,128)(2,1)}), bf16[128,512]{1,0:T(8,128)(2,1)}) %reduce-scatter.11.cloned.1.call-update) | async-done | bytes 131088 | tf_op jit(solution)/shard_map/reduce_scatter | solution.py:182
  121.0 0.9 add_convert_fusion.1
  121.9 15.6 %all_gather.13 = bf16[512,512]{1,0:T(8,128)(2,1)S(1)} all-gather(bf16[128,512]{1,0:T(8,128)(2,1)S(1)} %add_convert_fusion.1), channel_id=1, replica_groups=mesh['grp'=2,'tp'=4,'dp'=4] {'tp'}, dimensions={0}, use_global_device_ids=true | all-gather | bytes 655360 | tf_op jit(solution)/shard_map/all_gather | solution.py:195
  137.8 1.2 collective-permute-done.2
  139.0 1.6 collective-permute-start.3
  140.6 2.3 collective-permute-done.3
  143.1 2.0 fusion.13
  145.1 2.0 fusion.12
  147.5 2.5 copy.281
  150.1 0.6 copy-done.46
  150.7 0.7 copy.228
  151.8 28.0 %reduce-scatter.17.cloned.1.call-done = bf16[16,16384]{1,0:T(8,128)(2,1)} async-done(((bf16[64,16384]{1,0:T(8,128)(2,1)}), bf16[16,16384]{1,0:T(8,128)(2,1)}) %reduce-scatter.17.cloned.1.call-update) | async-done | bytes 524304
  179.8 1.4 copy.282
  181.1 0.7 fusion.158
  182.0 0.9 reshape.309
  183.5 1.4 convolution_convert_fusion.8
  184.9 1.4 convolution_convert_fusion.7
  186.4 1.5 convolution_convert_fusion.6
  187.9 1.8 fusion.74
  189.7 1.8 fusion.75
  191.7 2.8 reduce_window_sum.18
  195.2 7.1 %fusion = f32[16,4,8,256]{3,2,1,0:T(8,128)S(1)} fusion(f32[2,16,4,256,256]{4,3,2,1,0:T(8,128)} %param.38, bf16[4,16,8,256]{3,2,1,0:T(8,128)(2,1)} %copy-done.1), kind=kOutput, calls=%fused_computation.4 | convolution fusion | flops 67108864 | bytes 9175040 | tf_op jit(solution)/shard_map/bhtd,bhde->bhte/dot_general | solution.py:92
  202.3 1.2 gather_fusion
  203.5 1.2 gather_fusion.1
  205.3 0.8 copy.250
  206.8 1.7 bitcast_multiply_fusion.3
  208.6 1.5 fusion.109
  211.5 0.9 copy.227
  212.7 0.6 pad_maximum_fusion.12
  213.3 10.9 %fusion.3 = f32[1,16,4,256,256]{4,3,2,1,0:T(8,128)} fusion(f32[2,16,4,256,256]{4,3,2,1,0:T(8,128)} %param.38, f32[16,4]{1,0:T(8,128)S(1)} %copy.242, bf16[16,4,8,256]{3,2,0,1:T(8,128)(2,1)S(1)} %get-tuple-element.27, bf16[4,16,8,256]{3,2,1,0:T(8,128)(2,1)S(1)} %copy-done.9), kind=kOutput, calls=%fused_computation.7 | convolution fusion | flops 75497472 | bytes 34078976 | tf_op jit(solution)/shard_map/bhs,bhsd,bhse->bhde/dot_general | solution.py:104
  224.2 10.9 %fusion.7 = f32[1,16,4,256,256]{4,3,2,1,0:T(8,128)} fusion(f32[2,16,4,256,256]{4,3,2,1,0:T(8,128)} %param.38, f32[16,4]{1,0:T(8,128)S(1)} %copy.234, bf16[16,4,8,256]{3,2,0,1:T(8,128)(2,1)S(1)} %get-tuple-element.25, bf16[4,16,8,256]{3,2,1,0:T(8,128)(2,1)S(1)} %copy-done.7), kind=kOutput, calls=%fused_computation.12 | convolution fusion | flops 75497472 | bytes 34078976 | tf_op jit(solution)/shard_map/bhs,bhsd,bhse->bhde/dot_general | solution.py:104
  235.0 3.0 %convolution_convert_fusion.4 = bf16[512,512]{1,0:T(8,128)(2,1)} fusion(bf16[64,8,1024]{2,1,0:T(8,128)(2,1)} %all-gather.5.cloned.1.call-done, bf16[2,1024,512]{2,1,0:T(8,128)(2,1)} %param.36), kind=kOutput, calls=%fused_computation.28 | convolution fusion | flops 537133056 | bytes 2621440 | tf_op jit(solution)/shard_map/dot_general | solution.py:179
  238.1 23.1 %pad_maximum_fusion = f32[2,16,4,256,256]{4,3,2,1,0:T(8,128)} fusion(f32[1,16,4,256,256]{4,3,2,1,0:T(8,128)} %fusion.3, f32[1,16,4,256,256]{4,3,2,1,0:T(8,128)} %fusion.7), kind=kLoop, calls=%fused_computation.2 | loop fusion | flops 8388608 | bytes 67108864 | tf_op jit(solution)/shard_map/stack | solution.py:251
  261.2 0.9 add_convert_fusion
  262.1 15.5 %all_gather.15 = bf16[512,512]{1,0:T(8,128)(2,1)S(1)} all-gather(bf16[128,512]{1,0:T(8,128)(2,1)S(1)} %add_convert_fusion), channel_id=1, replica_groups=mesh['grp'=2,'tp'=4,'dp'=4] {'tp'}, dimensions={0}, use_global_device_ids=true | all-gather | bytes 655360 | tf_op jit(solution)/shard_map/all_gather | solution.py:195
  277.6 0.8 copy.380
  (192 shorter events, 12.9 us)
Async XLA Ops:
  7.2 9.7 %copy-start = (bf16[64,8,512]{2,1,0:T(8,128)(2,1)S(1)}, bf16[64,8,512]{2,1,0:T(8,128)(2,1)}, u32[]{:S(2)}) copy-start(bf16[64,8,512]{2,1,0:T(8,128)(2,1)} %param.21) | copy-start | bytes 1572868
  7.2 9.7 %copy-start.47 = (bf16[2,512,1024]{2,1,0:T(8,128)(2,1)S(1)}, bf16[2,512,1024]{2,1,0:T(8,128)(2,1)}, u32[]{:S(2)}) copy-start(bf16[2,512,1024]{2,1,0:T(8,128)(2,1)} %param.24) | copy-start | bytes 6291460
  7.2 46.7 %reduce-scatter.15.cloned.1.call-start = ((), (), s32[]{:S(2)}) async-start(), calls=%async_computation.8 | async-start | bytes 2621440
  8.6 1.4 collective-permute-start
  10.0 4.7 %collective-permute-start.1 = (f32[64,8]{1,0:T(8,128)S(1)}, f32[64,8]{1,0:T(8,128)S(1)}, u32[]{:S(2)}, u32[]{:S(2)}) collective-permute-start(f32[64,8]{1,0:T(8,128)S(1)} %add.281), channel_id=1, source_target_pairs={{0,2},{1,3},{2,0},{3,1},{4,6},{5,7},{6,4},{7,5},{8,10},{9,11},{10,... | collective-permute-start | bytes 6152 | tf_op jit(solution)/shard_map/ppermute | solution.py:18
  20.7 0.7 copy-start.45
  20.7 0.8 copy-start.24
  20.7 1.4 copy-start.43
  20.7 2.0 copy-start.44
  20.7 2.4 copy-start.32
  20.7 3.0 %copy-start.33 = (f32[2,1024]{1,0:T(2,128)S(1)}, f32[2,1024]{1,0:T(2,128)}, u32[]{:S(2)}) copy-start(f32[2,1024]{1,0:T(2,128)} %param.35) | copy-start | bytes 24580
  20.7 3.6 %copy-start.26 = (bf16[2,4,768]{2,1,0:T(4,128)(2,1)S(1)}, bf16[2,4,768]{2,1,0:T(4,128)(2,1)}, u32[]{:S(2)}) copy-start(bf16[2,4,768]{2,1,0:T(4,128)(2,1)} %param.30) | copy-start | bytes 36868
  20.7 4.2 %copy-start.27 = (bf16[2,4,768]{2,1,0:T(4,128)(2,1)S(1)}, bf16[2,4,768]{2,1,0:T(4,128)(2,1)}, u32[]{:S(2)}) copy-start(bf16[2,4,768]{2,1,0:T(4,128)(2,1)} %param.31) | copy-start | bytes 36868
  20.7 4.8 %copy-start.14 = (f32[2,4,1024]{2,1,0:T(4,128)S(1)}, f32[2,4,1024]{2,1,0:T(4,128)}, u32[]{:S(2)}) copy-start(f32[2,4,1024]{2,1,0:T(4,128)} %param.26) | copy-start | bytes 98308
  20.7 5.4 %copy-start.11 = (bf16[2,16,3,1024]{3,1,2,0:T(8,128)(2,1)S(1)}, bf16[2,16,3,1024]{3,1,2,0:T(8,128)(2,1)}, u32[]{:S(2)}) copy-start(bf16[2,16,3,1024]{3,1,2,0:T(8,128)(2,1)} %param.37) | copy-start | bytes 589828
  20.8 75.2 %all-gather.3.cloned.1.call-start = ((), (), s32[]{:S(2)}) async-start(), calls=%async_computation.4 | async-start | bytes 1310720 | tf_op jit(solution)/shard_map/all_gather | solution.py:177
  21.3 34.0 %copy-start.28 = (pred[16,8]{0,1:T(8,128)(4,1)}, pred[16,8]{0,1:T(8,128)(4,1)S(1)}, u32[]{:S(2)}) copy-start(pred[16,8]{0,1:T(8,128)(4,1)S(1)} %iota_compare_fusion.1) | copy-start | bytes 388
  22.1 43.7 %copy-start.39 = (pred[8,8]{1,0:T(8,128)(4,1)}, pred[8,8]{1,0:T(8,128)(4,1)S(1)}, u32[]{:S(2)}) copy-start(pred[8,8]{1,0:T(8,128)(4,1)S(1)} %iota_compare_fusion) | copy-start | bytes 196
  22.6 43.1 %copy-start.38 = (f32[4]{0:T(128)}, f32[4]{0:T(128)S(1)}, u32[]{:S(2)}) copy-start(f32[4]{0:T(128)S(1)} %get-tuple-element.66) | copy-start | bytes 52
  53.9 3.0 %copy-start.3 = (bf16[2,4,256,256]{3,2,1,0:T(8,128)(2,1)S(1)}, bf16[2,4,256,256]{3,2,1,0:T(8,128)(2,1)}, u32[]{:S(2)}) copy-start(bf16[2,4,256,256]{3,2,1,0:T(8,128)(2,1)} %param.27) | copy-start | bytes 3145732
  56.8 1.7 copy-start.10
  56.8 1.7 copy-start.48
  59.0 16.6 %copy-start.6 = (bf16[4,16,8,256]{3,2,1,0:T(8,128)(2,1)}, bf16[4,16,8,256]{3,2,1,0:T(8,128)(2,1)S(1)}, u32[]{:S(2)}) copy-start(bf16[4,16,8,256]{3,2,1,0:T(8,128)(2,1)S(1)} %convolution_convert_fusion.9) | copy-start | bytes 786436
  65.8 0.6 copy-start.12
  66.9 8.6 %copy-start.15 = (f32[16,4,1]{0,1,2:T(4,128)}, f32[16,4,1]{0,1,2:T(4,128)S(1)}, u32[]{:S(2)}) copy-start(f32[16,4,1]{0,1,2:T(4,128)S(1)} %copy.232) | copy-start | bytes 772
  68.6 7.0 %copy-start.13 = (f32[16,4,8]{2,1,0:T(4,128)S(1)}, f32[16,4,8]{2,1,0:T(4,128)}, u32[]{:S(2)}) copy-start(f32[16,4,8]{2,1,0:T(4,128)} %copy-done.12) | copy-start | bytes 6148
  75.6 1.8 copy-start.23
  77.0 0.7 copy-start.29
  79.1 41.9 %reduce-scatter.11.cloned.1.call-start = ((), (), s32[]{:S(2)}) async-start(), calls=%async_computation.5 | async-start | bytes 655360 | tf_op jit(solution)/shard_map/reduce_scatter | solution.py:182
  99.0 44.1 %copy-start.42 = (f32[1,512]{1,0:T(1,128)S(1)}, f32[1,512]{1,0:T(1,128)}, u32[]{:S(2)}) copy-start(f32[1,512]{1,0:T(1,128)} %get-tuple-element.60) | copy-start | bytes 6148
  99.0 80.8 %reduce-scatter.17.cloned.1.call-start = ((), (), s32[]{:S(2)}) async-start(), calls=%async_computation.9 | async-start | bytes 2621440
  137.8 1.3 collective-permute-start.2
  139.0 3.9 %collective-permute-start.3 = (f32[64,8]{1,0:T(8,128)S(1)}, f32[64,8]{1,0:T(8,128)S(1)}, u32[]{:S(2)}, u32[]{:S(2)}) collective-permute-start(f32[64,8]{1,0:T(8,128)S(1)} %add.307), channel_id=1, source_target_pairs={{0,2},{1,3},{2,0},{3,1},{4,6},{5,7},{6,4},{7,5},{8,10},{9,11},{10,... | collective-permute-start | bytes 6152 | tf_op jit(solution)/shard_map/ppermute | solution.py:18
  150.0 0.7 copy-start.46
  150.0 1.3 copy-start.34
  150.0 85.0 %all-gather.5.cloned.1.call-start = ((), (), s32[]{:S(2)}) async-start(), calls=%async_computation.6 | async-start | bytes 1310720 | tf_op jit(solution)/shard_map/all_gather | solution.py:177
  179.8 3.2 %copy-start.17 = (f32[1,1,1024]{2,1,0:T(1,128)S(1)}, f32[1,1,1024]{2,1,0:T(1,128)}, u32[]{:S(2)}) copy-start(f32[1,1,1024]{2,1,0:T(1,128)} %get-tuple-element.37) | copy-start | bytes 12292
  179.8 3.2 %copy-start.18 = (f32[1,1,1024]{2,1,0:T(1,128)S(1)}, f32[1,1,1024]{2,1,0:T(1,128)}, u32[]{:S(2)}) copy-start(f32[1,1,1024]{2,1,0:T(1,128)} %get-tuple-element.38) | copy-start | bytes 12292
  179.8 3.2 %copy-start.19 = (f32[1,1,1024]{2,1,0:T(1,128)S(1)}, f32[1,1,1024]{2,1,0:T(1,128)}, u32[]{:S(2)}) copy-start(f32[1,1,1024]{2,1,0:T(1,128)} %get-tuple-element.43) | copy-start | bytes 12292
  179.8 3.2 %copy-start.20 = (f32[1,1,1024]{2,1,0:T(1,128)S(1)}, f32[1,1,1024]{2,1,0:T(1,128)}, u32[]{:S(2)}) copy-start(f32[1,1,1024]{2,1,0:T(1,128)} %get-tuple-element.44) | copy-start | bytes 12292
  183.3 4.6 %copy-start.35 = (bf16[4,768,1,1]{1,0,2,3:T(4,128)(2,1)S(1)}, bf16[4,768,1,1]{1,0,2,3:T(4,128)(2,1)}, u32[]{:S(2)}) copy-start(bf16[4,768,1,1]{1,0,2,3:T(4,128)(2,1)} %get-tuple-element.49) | copy-start | bytes 18436
  183.5 2.9 %copy-start.49 = (bf16[2,4,256,256]{3,2,1,0:T(8,128)(2,1)S(1)}, bf16[2,4,256,256]{3,2,1,0:T(8,128)(2,1)}, u32[]{:S(2)}) copy-start(bf16[2,4,256,256]{3,2,1,0:T(8,128)(2,1)} %param.29) | copy-start | bytes 3145732
  184.9 4.8 %copy-start.1 = (bf16[4,16,8,256]{3,2,1,0:T(8,128)(2,1)}, bf16[4,16,8,256]{3,2,1,0:T(8,128)(2,1)S(1)}, u32[]{:S(2)}) copy-start(bf16[4,16,8,256]{3,2,1,0:T(8,128)(2,1)S(1)} %convolution_convert_fusion.8) | copy-start | bytes 786436
  186.4 5.2 %copy-start.4 = (bf16[4,16,8,256]{3,2,1,0:T(8,128)(2,1)}, bf16[4,16,8,256]{3,2,1,0:T(8,128)(2,1)S(1)}, u32[]{:S(2)}) copy-start(bf16[4,16,8,256]{3,2,1,0:T(8,128)(2,1)S(1)} %convolution_convert_fusion.7) | copy-start | bytes 786436
  186.4 3.4 %copy-start.36 = (bf16[4,768,1,1]{1,0,2,3:T(4,128)(2,1)S(1)}, bf16[4,768,1,1]{1,0,2,3:T(4,128)(2,1)}, u32[]{:S(2)}) copy-start(bf16[4,768,1,1]{1,0,2,3:T(4,128)(2,1)} %get-tuple-element.47) | copy-start | bytes 18436
  187.9 3.7 %copy-start.8 = (bf16[4,16,8,256]{3,2,1,0:T(8,128)(2,1)}, bf16[4,16,8,256]{3,2,1,0:T(8,128)(2,1)S(1)}, u32[]{:S(2)}) copy-start(bf16[4,16,8,256]{3,2,1,0:T(8,128)(2,1)S(1)} %convolution_convert_fusion.6) | copy-start | bytes 786436
  187.9 3.7 %copy-start.41 = (f32[4]{0:T(128)S(1)}, f32[4]{0:T(128)}, u32[]{:S(2)}) copy-start(f32[4]{0:T(128)} %get-tuple-element.63) | copy-start | bytes 52
  187.9 6.7 %copy-start.37 = (f32[4]{0:T(128)S(1)}, f32[4]{0:T(128)}, u32[]{:S(2)}) copy-start(f32[4]{0:T(128)} %get-tuple-element.65) | copy-start | bytes 52
  187.9 6.7 %copy-start.40 = (pred[8,8]{1,0:T(8,128)(4,1)S(1)}, pred[8,8]{1,0:T(8,128)(4,1)}, u32[]{:S(2)}) copy-start(pred[8,8]{1,0:T(8,128)(4,1)} %copy-done.39) | copy-start | bytes 196
  202.3 2.6 copy-start.31
  202.3 4.1 %copy-start.16 = (f32[16,4,1]{0,1,2:T(4,128)S(1)}, f32[16,4,1]{0,1,2:T(4,128)}, u32[]{:S(2)}) copy-start(f32[16,4,1]{0,1,2:T(4,128)} %copy-done.15) | copy-start | bytes 772
  202.3 4.1 %copy-start.25 = (f32[2,16,4]{1,2,0:T(4,128)S(1)}, f32[2,16,4]{1,2,0:T(4,128)}, u32[]{:S(2)}) copy-start(f32[2,16,4]{1,2,0:T(4,128)} %param.39) | copy-start | bytes 1540
  203.5 5.0 %copy-start.2 = (bf16[4,16,8,256]{3,2,1,0:T(8,128)(2,1)S(1)}, bf16[4,16,8,256]{3,2,1,0:T(8,128)(2,1)}, u32[]{:S(2)}) copy-start(bf16[4,16,8,256]{3,2,1,0:T(8,128)(2,1)} %copy-done.1) | copy-start | bytes 786436
  208.6 1.9 copy-start.22
  210.1 1.0 copy-start.5
  210.1 0.9 copy-start.21
  210.1 0.9 copy-start.30
  210.5 2.8 copy-start.9
  212.4 48.8 %reduce-scatter.13.cloned.1.call-start = ((), (), s32[]{:S(2)}) async-start(), calls=%async_computation.7 | async-start | bytes 655360 | tf_op jit(solution)/shard_map/reduce_scatter | solution.py:182
  213.3 10.9 %copy-start.7 = (bf16[4,16,8,256]{3,2,1,0:T(8,128)(2,1)S(1)}, bf16[4,16,8,256]{3,2,1,0:T(8,128)(2,1)}, u32[]{:S(2)}) copy-start(bf16[4,16,8,256]{3,2,1,0:T(8,128)(2,1)} %copy-done.6) | copy-start | bytes 786436
Sparse Core Ops, SparseCore 0:
  20.9 32.9 reduce-scatter.14
  79.2 16.6 all-gather.2
  99.2 21.8 reduce-scatter.10
  150.2 29.5 reduce-scatter.16
  212.5 16.7 all-gather.4
  238.2 21.9 reduce-scatter.12
